TPU v7x, 32 devices: a whole 2x2x4 slice. The times are simulated.
32 devices in a mesh: sp: 8 (over z, y), tp: 4 (over x, core).
Axes of the slice: x: 2, y: 2, z: 4, core: 2. Of those that a mesh axis runs over, the one named last changes fastest.
Arguments:
- hidden_states: bfloat16 [2048, 4096], P('sp', 'tp'), may hold values from -6 to 6
- norm_gain: float32 [4096], replicated, may hold values from 0.1 to 1.9
- query_weight: bfloat16 [4096, 2048], P('sp', 'tp'), may hold values from -0.09375 to 0.09375
- key_weight: bfloat16 [4096, 2048], P('sp', 'tp'), may hold values from -0.09375 to 0.09375
- value_weight: bfloat16 [4096, 2048], P('sp', 'tp'), may hold values from -0.09375 to 0.09375
- output_gate_weight: bfloat16 [4096, 2048], P('sp', 'tp'), may hold values from -0.09375 to 0.09375
- unit_input_weight: bfloat16 [4096, 2048], P('sp', 'tp'), may hold values from -0.09375 to 0.09375
- unit_gate_weight: bfloat16 [4096, 2048], P('sp', 'tp'), may hold values from -0.09375 to 0.09375
- decay_forward: float32 [16], P('tp'), may hold values from 0 to 16
- decay_backward: float32 [16], P('tp'), may hold values from 0 to 16
- group_gain: float32 [2048], P('tp'), may hold values from 0.1 to 1.9
- group_bias: float32 [2048], P('tp'), may hold values from -3 to 3
- depth_kernel: float32 [31, 2048], P(None, 'tp'), may hold values from -7 to 7
- depth_bias: float32 [2048], P('tp'), may hold values from -3 to 3
- channel_gain: float32 [2048], P('tp'), may hold values from 0.1 to 1.9
- channel_bias: float32 [2048], P('tp'), may hold values from -3 to 3
- retention_out_weight: bfloat16 [2048, 4096], P('tp', 'sp'), may hold values from -0.09375 to 0.09375
- convolution_out_weight: bfloat16 [2048, 4096], P('tp', 'sp'), may hold values from -0.09375 to 0.09375
Outputs:
- mixed_out: bfloat16 [2048, 4096], P(('sp', 'tp'))
All inputs are finite; a program needn't handle non-finite values.
Results may differ from a plain program's by a relative error of at most 0.018.
Values may be sent and summed in bfloat16 or wider, within the bound.
A program may use at most 128 MiB of HBM per device.

v0:
```python
import jax
import jax.numpy as jnp
from jax import lax
from jax.sharding import PartitionSpec as P

HEAD_DIM = 128
CONV_WIDTH = 2048
KERNEL = 31
BLOCK = 128
EPS = 1e-06
THETA = 10000.0


def with_halo(cells, sides, width):
    for axis, dim in sides:
        count = lax.axis_size(axis)
        ends = count - 1
        head = lax.slice_in_dim(cells, 0, width, axis=dim)
        tail = lax.slice_in_dim(cells, cells.shape[dim] - width, cells.shape[dim], axis=dim)
        cells = jnp.concatenate(
            [
                lax.ppermute(tail, axis, [(i, (i + 1) % count) for i in range(ends)]),
                cells,
                lax.ppermute(head, axis, [((i + 1) % count, i) for i in range(ends)]),
            ],
            axis=dim,
        )
    return cells


def rotate(rows, positions):
    half_dim = rows.shape[-1] // 2
    inverse = THETA ** (-jnp.arange(half_dim, dtype=jnp.float32) / half_dim)
    angles = positions.astype(jnp.float32)[:, None] * inverse[None, :]
    cosine = jnp.cos(angles)[:, None, :]
    sine = jnp.sin(angles)[:, None, :]
    widened = rows.astype(jnp.float32)
    first_half = widened[..., :half_dim]
    second_half = widened[..., half_dim:]
    turned = jnp.concatenate(
        [first_half * cosine - second_half * sine, second_half * cosine + first_half * sine],
        axis=-1,
    )
    return turned.astype(jnp.bfloat16)


def to_blocks(rows):
    return rows.reshape(rows.shape[0] // BLOCK, BLOCK, rows.shape[1], rows.shape[2]).transpose(
        2, 0, 1, 3
    )


def from_blocks(blocks):
    return blocks.transpose(1, 2, 0, 3).reshape(
        blocks.shape[1] * blocks.shape[2], blocks.shape[0], blocks.shape[3]
    )


def blockwise(queries, key_rows, values, log_decay, include_diag):
    block_len = queries.shape[2]
    position = jnp.arange(block_len, dtype=jnp.float32)
    distance = position[:, None] - position[None, :]
    allowed = distance >= 0 if include_diag else distance > 0
    inside = jnp.where(
        allowed[None], jnp.exp(log_decay[:, None, None] * jnp.maximum(distance, 0.0)[None]), 0.0
    )
    query_wide = queries.astype(jnp.float32)
    key_wide = key_rows.astype(jnp.float32)
    value_wide = values.astype(jnp.float32)
    scores = (
        jnp.einsum("hnqd,hnkd->hnqk", query_wide, key_wide, precision=lax.Precision.HIGHEST)
        * inside[:, None]
    )
    inner_part = jnp.einsum("hnqk,hnkd->hnqd", scores, value_wide, precision=lax.Precision.HIGHEST)
    toward_end = jnp.exp(log_decay[:, None] * (block_len - 1.0 - position)[None])
    block_states = jnp.einsum(
        "hnkd,hnke->hnde",
        key_wide * toward_end[:, None, :, None],
        value_wide,
        precision=lax.Precision.HIGHEST,
    )
    block_decay = jnp.exp(log_decay * block_len)[:, None, None]

    def advance(state_now, block_state):
        return (block_decay * state_now + block_state, state_now)

    initial = jnp.zeros(
        (block_states.shape[0], block_states.shape[2], block_states.shape[3]), jnp.float32
    )
    final_state, earlier = lax.scan(advance, initial, jnp.moveaxis(block_states, 1, 0))
    earlier = jnp.moveaxis(earlier, 0, 1)
    from_start = jnp.exp(log_decay[:, None] * (position + 1.0)[None])
    cross_part = jnp.einsum(
        "hnqd,hnde->hnqe",
        query_wide * from_start[:, None, :, None],
        earlier,
        precision=lax.Precision.HIGHEST,
    )
    return (inner_part + cross_part, final_state)


def group_norm(retained, group_gain, group_bias, gate_rows):
    row_mean = jnp.mean(retained, axis=-1, keepdims=True)
    centered = retained - row_mean
    variance = jnp.mean(centered * centered, axis=-1, keepdims=True)
    scaled = (centered * lax.rsqrt(variance + EPS)).reshape(retained.shape[0], -1)
    scaled = scaled * group_gain[None, :] + group_bias[None, :]
    return (jax.nn.silu(gate_rows.astype(jnp.float32)) * scaled).astype(jnp.bfloat16)


def shards(
    hidden_states,
    norm_gain,
    query_weight,
    key_weight,
    value_weight,
    output_gate_weight,
    unit_input_weight,
    unit_gate_weight,
    decay_forward,
    decay_backward,
    group_gain,
    group_bias,
    depth_kernel,
    depth_bias,
    channel_gain,
    channel_bias,
    retention_out_weight,
    convolution_out_weight,
):
    row_total = hidden_states.shape[0]
    whole = lax.all_gather(hidden_states, "tp", axis=1, tiled=True)
    widened = whole.astype(jnp.float32)
    normed = (
        widened
        * lax.rsqrt(jnp.mean(widened * widened, axis=-1, keepdims=True) + EPS)
        * norm_gain[None, :]
    ).astype(jnp.bfloat16)
    slabs = (
        lax.all_gather(query_weight, "sp", axis=0, tiled=True),
        lax.all_gather(key_weight, "sp", axis=0, tiled=True),
        lax.all_gather(value_weight, "sp", axis=0, tiled=True),
        lax.all_gather(output_gate_weight, "sp", axis=0, tiled=True),
        lax.all_gather(unit_input_weight, "sp", axis=0, tiled=True),
        lax.all_gather(unit_gate_weight, "sp", axis=0, tiled=True),
    )
    summed = tuple((jnp.dot(normed, slab, preferred_element_type=jnp.float32) for slab in slabs))
    proj_q, proj_k, proj_v, proj_g, proj_a, proj_b = tuple(
        (part_sum.astype(jnp.bfloat16) for part_sum in summed)
    )
    head_count = proj_q.shape[1] // HEAD_DIM
    device = lax.axis_index("sp")
    positions = device * row_total + jnp.arange(row_total, dtype=jnp.int32)
    queries = rotate(proj_q.reshape(row_total, head_count, HEAD_DIM), positions)
    key_rows = rotate(proj_k.reshape(row_total, head_count, HEAD_DIM), positions)
    values = proj_v.reshape(row_total, head_count, HEAD_DIM)
    log_forward = jax.nn.log_sigmoid(decay_forward)
    log_backward = jax.nn.log_sigmoid(decay_backward)
    ahead_local, state_ahead = blockwise(
        to_blocks(queries), to_blocks(key_rows), to_blocks(values), log_forward, True
    )
    behind_local, state_behind = blockwise(
        to_blocks(queries[::-1]),
        to_blocks(key_rows[::-1]),
        to_blocks(values[::-1]),
        log_backward,
        False,
    )
    slabs = (
        lax.all_gather(state_ahead[None].astype(jnp.bfloat16), "sp", axis=0, tiled=True).astype(
            jnp.float32
        ),
        lax.all_gather(state_behind[None].astype(jnp.bfloat16), "sp", axis=0, tiled=True).astype(
            jnp.float32
        ),
    )
    source = jnp.arange(slabs[0].shape[0], dtype=jnp.int32)
    gap_ahead = device - 1 - source
    gap_behind = source - device - 1
    weight_ahead = jnp.where(
        gap_ahead[:, None] >= 0,
        jnp.exp(
            log_forward[None, :]
            * row_total
            * jnp.maximum(gap_ahead, 0).astype(jnp.float32)[:, None]
        ),
        0.0,
    )
    weight_behind = jnp.where(
        gap_behind[:, None] >= 0,
        jnp.exp(
            log_backward[None, :]
            * row_total
            * jnp.maximum(gap_behind, 0).astype(jnp.float32)[:, None]
        ),
        0.0,
    )
    enter_ahead = jnp.zeros_like(state_ahead) + jnp.einsum(
        "jh,jhde->hde", weight_ahead, slabs[0], precision=lax.Precision.HIGHEST
    )
    enter_behind = jnp.zeros_like(state_behind) + jnp.einsum(
        "jh,jhde->hde", weight_behind, slabs[1], precision=lax.Precision.HIGHEST
    )
    local_position = jnp.arange(row_total, dtype=jnp.float32)
    lift_ahead = jnp.exp(log_forward[None, :] * (local_position + 1.0)[:, None])
    lift_behind = jnp.exp(log_backward[None, :] * (row_total - local_position)[:, None])
    query_wide = queries.astype(jnp.float32)
    carried = jnp.einsum(
        "shd,hde->she",
        query_wide * lift_ahead[:, :, None],
        enter_ahead,
        precision=lax.Precision.HIGHEST,
    )
    carried = carried + jnp.einsum(
        "shd,hde->she",
        query_wide * lift_behind[:, :, None],
        enter_behind,
        precision=lax.Precision.HIGHEST,
    )
    retained = from_blocks(ahead_local) + from_blocks(behind_local)[::-1] + carried
    retention_rows = group_norm(retained, group_gain, group_bias, proj_g)
    unit = (proj_a.astype(jnp.float32) * jax.nn.sigmoid(proj_b.astype(jnp.float32))).astype(
        jnp.bfloat16
    )
    half_kernel = (KERNEL - 1) // 2
    padded = with_halo(unit, (("sp", 0),), half_kernel)
    filtered = jnp.broadcast_to(depth_bias[None, :], (row_total, unit.shape[1]))
    for offset in range(KERNEL):
        filtered = filtered + depth_kernel[offset][None, :] * padded[
            offset : offset + row_total
        ].astype(jnp.float32)
    row_sum, row_squares = lax.psum(
        (jnp.sum(filtered, axis=1), jnp.sum(filtered * filtered, axis=1)), "tp"
    )
    row_mean = (row_sum / CONV_WIDTH)[:, None]
    variance = (row_squares / CONV_WIDTH)[:, None] - row_mean * row_mean
    leveled = (filtered - row_mean) * lax.rsqrt(variance + EPS) * channel_gain[
        None, :
    ] + channel_bias[None, :]
    convolution_rows = jax.nn.silu(leveled).astype(jnp.bfloat16)
    retention_full, convolution_full = (
        lax.all_gather(retention_out_weight, "sp", axis=1, tiled=True),
        lax.all_gather(convolution_out_weight, "sp", axis=1, tiled=True),
    )
    return lax.psum_scatter(
        (
            jnp.dot(retention_rows, retention_full, preferred_element_type=jnp.float32)
            + jnp.dot(convolution_rows, convolution_full, preferred_element_type=jnp.float32)
        ).astype(jnp.bfloat16),
        "tp",
        scatter_dimension=0,
        tiled=True,
    )


def solution(mesh):
    placed = (
        P("sp", "tp"),
        P(),
        P("sp", "tp"),
        P("sp", "tp"),
        P("sp", "tp"),
        P("sp", "tp"),
        P("sp", "tp"),
        P("sp", "tp"),
        P("tp"),
        P("tp"),
        P("tp"),
        P("tp"),
        P(None, "tp"),
        P("tp"),
        P("tp"),
        P("tp"),
        P("tp", "sp"),
        P("tp", "sp"),
    )
    return jax.shard_map(
        shards, mesh=mesh, in_specs=placed, out_specs=P(("sp", "tp"), None), check_vma=False
    )
```

profile of v0, /device:TPU:0, one launch (start us, length us, event | category | flops | bytes accessed | tf_op | source)
XLA Modules:
  0.0 751.1 jit_solution(1209921822257919842)
XLA Ops:
  10.6 1.2 broadcast_multiply_fusion.2
  12.4 1.2 multiply_cosine_fusion
  13.6 20.6 %all-gather.14.cloned.1.call-done = bf16[256,4096]{1,0:T(8,128)(2,1)} async-done(((bf16[256,1024]{1,0:T(8,128)(2,1)}), bf16[256,4096]{1,0:T(8,128)(2,1)}) %all-gather.14.cloned.1.call-update) | async-done | bytes 2097168 | tf_op jit(solution)/shard_map/all_gather | solution.py:132
  34.2 2.1 fusion.1
  36.3 72.8 %all-gather.18.cloned.1.call-done = bf16[4096,512]{1,0:T(8,128)(2,1)} async-done(((bf16[512,512]{1,0:T(8,128)(2,1)}), bf16[4096,512]{1,0:T(8,128)(2,1)}) %all-gather.18.cloned.1.call-update) | async-done | bytes 4194320 | tf_op jit(solution)/shard_map/all_gather | solution.py:140
  109.2 4.1 fusion.15
  113.5 69.2 %all-gather.20.cloned.1.call-done = bf16[4096,512]{1,0:T(8,128)(2,1)} async-done(((bf16[512,512]{1,0:T(8,128)(2,1)}), bf16[4096,512]{1,0:T(8,128)(2,1)}) %all-gather.20.cloned.1.call-update) | async-done | bytes 4194320 | tf_op jit(solution)/shard_map/all_gather | solution.py:141
  182.7 3.5 fusion.14
  188.0 68.0 %all-gather.22.cloned.1.call-done = bf16[4096,512]{1,0:T(8,128)(2,1)} async-done(((bf16[512,512]{1,0:T(8,128)(2,1)}), bf16[4096,512]{1,0:T(8,128)(2,1)}) %all-gather.22.cloned.1.call-update) | async-done | bytes 4194320 | tf_op jit(solution)/shard_map/all_gather | solution.py:142
  256.0 4.1 convolution_convert_fusion.2
  267.1 0.8 exponential_select_fusion
  268.4 61.0 %all-gather.26.cloned.1.call-done = bf16[4096,512]{1,0:T(8,128)(2,1)} async-done(((bf16[512,512]{1,0:T(8,128)(2,1)}), bf16[4096,512]{1,0:T(8,128)(2,1)}) %all-gather.26.cloned.1.call-update) | async-done | bytes 4194320 | tf_op jit(solution)/shard_map/all_gather | solution.py:144
  329.4 4.9 fusion.13
  334.3 68.4 %all-gather.28.cloned.1.call-done = bf16[4096,512]{1,0:T(8,128)(2,1)} async-done(((bf16[512,512]{1,0:T(8,128)(2,1)}), bf16[4096,512]{1,0:T(8,128)(2,1)}) %all-gather.28.cloned.1.call-update) | async-done | bytes 4194320 | tf_op jit(solution)/shard_map/all_gather | solution.py:145
  402.7 4.3 fusion.12
  407.0 2.6 collective-permute-start
  409.6 1.5 collective-permute-start.1
  413.3 0.8 convolution_add_fusion.2
  415.6 3.7 fusion.97
  419.4 6.0 all-reduce
  425.4 18.2 %all-gather.34.cloned.1.call-done = bf16[32,128,128]{2,1,0:T(8,128)(2,1)} async-done(((bf16[4,128,128]{2,1,0:T(8,128)(2,1)}), bf16[32,128,128]{2,1,0:T(8,128)(2,1)}) %all-gather.34.cloned.1.call-update) | async-done | bytes 1048592 | tf_op jit(solution)/shard_map/all_gather | solution.py:173
  443.7 2.4 multiply_reduce_fusion
  446.1 38.7 %all-gather.32.cloned.1.call-done = bf16[32,128,128]{2,1,0:T(8,128)(2,1)} async-done(((bf16[4,128,128]{2,1,0:T(8,128)(2,1)}), bf16[32,128,128]{2,1,0:T(8,128)(2,1)}) %all-gather.32.cloned.1.call-update) | async-done | bytes 1048592 | tf_op jit(solution)/shard_map/all_gather | solution.py:170
  484.8 1.6 multiply_reduce_fusion.1
  486.4 0.8 fusion.17
  487.2 1.8 fusion.105
  489.4 69.1 %all-gather.16.cloned.1.call-done = bf16[4096,512]{1,0:T(8,128)(2,1)} async-done(((bf16[512,512]{1,0:T(8,128)(2,1)}), bf16[4096,512]{1,0:T(8,128)(2,1)}) %all-gather.16.cloned.1.call-update) | async-done | bytes 4194320 | tf_op jit(solution)/shard_map/all_gather | solution.py:143
  558.5 75.1 %all-gather.24.cloned.1.call-done = bf16[512,4096]{1,0:T(8,128)(2,1)} async-done(((bf16[512,512]{1,0:T(8,128)(2,1)}), bf16[512,4096]{1,0:T(8,128)(2,1)}) %all-gather.24.cloned.1.call-update) | async-done | bytes 4194320 | tf_op jit(solution)/shard_map/all_gather | solution.py:242
  633.6 8.0 %fusion.28 = f32[256,4096]{1,0:T(8,128)} fusion(bf16[512,4096]{1,0:T(8,128)(2,1)} %all-gather.24.cloned.1.call-done, f32[256,512]{1,0:T(8,128)S(1)} %copy.67, bf16[4096,512]{1,0:T(8,128)(2,1)} %all-gather.16.cloned.1.call-done, f32[512]{0:T(512)S(1)} %copy-done.43, f32[512]{0:T(512)S(1)} %copy-done.44, bf16[256,4096]{1,0:T(8,128)(2,1)S(1)} %copy-done.1, ...), kind=kOutput, calls=%fused_computation.89 | convolution fusion | flops 2152988672 | bytes 15225856 | tf_op jit(solution)/shard_map/dot_general | solution.py:247
  641.6 66.9 %all-gather.30.cloned.1.call-done = bf16[512,4096]{1,0:T(8,128)(2,1)} async-done(((bf16[512,512]{1,0:T(8,128)(2,1)}), bf16[512,4096]{1,0:T(8,128)(2,1)}) %all-gather.30.cloned.1.call-update) | async-done | bytes 4194320 | tf_op jit(solution)/shard_map/all_gather | solution.py:243
  708.5 6.2 fusion
  714.7 29.5 %reduce-scatter.2.cloned.1.call-done = bf16[64,4096]{1,0:T(8,128)(2,1)} async-done(((bf16[256,4096]{1,0:T(8,128)(2,1)}), bf16[64,4096]{1,0:T(8,128)(2,1)}) %reduce-scatter.2.cloned.1.call-update) | async-done | bytes 524304 | tf_op jit(solution)/shard_map/reduce_scatter | solution.py:245
  (185 shorter events, 17.9 us)
Async XLA Ops:
  6.5 102.6 %copy-start.38 = (f32[4096]{0:T(1024)S(1)}, f32[4096]{0:T(1024)}, u32[]{:S(2)}) copy-start(f32[4096]{0:T(1024)} %param.23) | copy-start | bytes 49156
  6.5 27.7 %all-gather.14.cloned.1.call-start = ((), (), s32[]{:S(2)}) async-start(), calls=%async_computation.1 | async-start | bytes 2621440 | tf_op jit(solution)/shard_map/all_gather | solution.py:132
  7.3 101.9 %all-gather.18.cloned.1.call-start = ((), (), s32[]{:S(2)}) async-start(), calls=%async_computation.3 | async-start | bytes 4718592 | tf_op jit(solution)/shard_map/all_gather | solution.py:140
  8.0 174.7 %all-gather.20.cloned.1.call-start = ((), (), s32[]{:S(2)}) async-start(), calls=%async_computation.4 | async-start | bytes 4718592 | tf_op jit(solution)/shard_map/all_gather | solution.py:141
  8.7 247.3 %all-gather.22.cloned.1.call-start = ((), (), s32[]{:S(2)}) async-start(), calls=%async_computation.5 | async-start | bytes 4718592 | tf_op jit(solution)/shard_map/all_gather | solution.py:142
  9.3 320.0 %all-gather.26.cloned.1.call-start = ((), (), s32[]{:S(2)}) async-start(), calls=%async_computation.7 | async-start | bytes 4718592 | tf_op jit(solution)/shard_map/all_gather | solution.py:144
  9.9 392.8 %all-gather.28.cloned.1.call-start = ((), (), s32[]{:S(2)}) async-start(), calls=%async_computation.8 | async-start | bytes 4718592 | tf_op jit(solution)/shard_map/all_gather | solution.py:145
  10.5 433.2 %all-gather.34.cloned.1.call-start = ((), (), s32[]{:S(2)}) async-start(), calls=%async_computation.12 | async-start | bytes 1179648 | tf_op jit(solution)/shard_map/all_gather | solution.py:173
  11.8 24.5 %copy-start.27 = (f32[4]{0:T(128)}, f32[4]{0:T(128)S(1)}, u32[]{:S(2)}) copy-start(f32[4]{0:T(128)S(1)} %get-tuple-element.208) | copy-start | bytes 52
  36.3 72.8 %copy-start.33 = (f32[256]{0:T(256)}, f32[256]{0:T(256)S(1)}, u32[]{:S(2)}) copy-start(f32[256]{0:T(256)S(1)} %add_rsqrt_fusion.2) | copy-start | bytes 3076
  36.3 146.4 %copy-start = (bf16[256,4096]{1,0:T(8,128)(2,1)S(1)}, bf16[256,4096]{1,0:T(8,128)(2,1)}, u32[]{:S(2)}) copy-start(bf16[256,4096]{1,0:T(8,128)(2,1)} %all-gather.14.cloned.1.call-done) | copy-start | bytes 6291460
  186.4 69.6 %copy-start.34 = (f32[256]{0:T(256)S(1)}, f32[256]{0:T(256)}, u32[]{:S(2)}) copy-start(f32[256]{0:T(256)} %copy-done.33) | copy-start | bytes 3076
  186.4 69.6 %copy-start.39 = (f32[4096]{0:T(1024)S(1)}, f32[4096]{0:T(1024)}, u32[]{:S(2)}) copy-start(f32[4096]{0:T(1024)} %param.23) | copy-start | bytes 49156
  261.9 222.9 %all-gather.32.cloned.1.call-start = ((), (), s32[]{:S(2)}) async-start(), calls=%async_computation.11 | async-start | bytes 1179648 | tf_op jit(solution)/shard_map/all_gather | solution.py:170
  263.2 66.2 %copy-start.35 = (f32[256]{0:T(256)S(1)}, f32[256]{0:T(256)}, u32[]{:S(2)}) copy-start(f32[256]{0:T(256)} %copy-done.33) | copy-start | bytes 3076
  263.2 66.2 %copy-start.40 = (f32[4096]{0:T(1024)S(1)}, f32[4096]{0:T(1024)}, u32[]{:S(2)}) copy-start(f32[4096]{0:T(1024)} %param.23) | copy-start | bytes 49156
  263.9 294.6 %all-gather.16.cloned.1.call-start = ((), (), s32[]{:S(2)}) async-start(), calls=%async_computation.2 | async-start | bytes 4718592 | tf_op jit(solution)/shard_map/all_gather | solution.py:143
  264.6 369.0 %all-gather.24.cloned.1.call-start = ((), (), s32[]{:S(2)}) async-start(), calls=%async_computation.6 | async-start | bytes 4718592 | tf_op jit(solution)/shard_map/all_gather | solution.py:242
  265.2 443.3 %all-gather.30.cloned.1.call-start = ((), (), s32[]{:S(2)}) async-start(), calls=%async_computation.9 | async-start | bytes 4718592 | tf_op jit(solution)/shard_map/all_gather | solution.py:243
  265.9 478.3 %reduce-scatter.2.cloned.1.call-start = ((), (), s32[]{:S(2)}) async-start(), calls=%async_computation.10 | async-start | bytes 2621440 | tf_op jit(solution)/shard_map/reduce_scatter | solution.py:245
  268.4 134.3 %copy-start.36 = (f32[256]{0:T(256)S(1)}, f32[256]{0:T(256)}, u32[]{:S(2)}) copy-start(f32[256]{0:T(256)} %copy-done.33) | copy-start | bytes 3076
  268.4 134.3 %copy-start.41 = (f32[4096]{0:T(1024)S(1)}, f32[4096]{0:T(1024)}, u32[]{:S(2)}) copy-start(f32[4096]{0:T(1024)} %param.23) | copy-start | bytes 49156
  407.0 8.2 %collective-permute-start = (bf16[15,512]{1,0:T(8,128)(2,1)S(1)}, bf16[15,512]{1,0:T(8,128)(2,1)S(1)}, u32[]{:S(2)}, u32[]{:S(2)}) collective-permute-start(bf16[15,512]{1,0:T(8,128)(2,1)S(1)} %get-tuple-element.158), channel_id=1, source_target_pairs={{0,4},{4,8},{8,12},{12,16},{16,20},{20,24},{24,28},{1,5},{5,9},{9,... | collective-permute-start | bytes 46088 | tf_op jit(solution)/shard_map/ppermute | solution.py:22
  409.6 5.9 collective-permute-start.1
  443.7 189.9 %copy-start.1 = (bf16[256,4096]{1,0:T(8,128)(2,1)S(1)}, bf16[256,4096]{1,0:T(8,128)(2,1)}, u32[]{:S(2)}) copy-start(bf16[256,4096]{1,0:T(8,128)(2,1)} %all-gather.14.cloned.1.call-done) | copy-start | bytes 6291460
  443.7 189.9 %copy-start.37 = (f32[256]{0:T(256)S(1)}, f32[256]{0:T(256)}, u32[]{:S(2)}) copy-start(f32[256]{0:T(256)} %copy-done.33) | copy-start | bytes 3076
  443.7 189.9 %copy-start.42 = (f32[4096]{0:T(1024)S(1)}, f32[4096]{0:T(1024)}, u32[]{:S(2)}) copy-start(f32[4096]{0:T(1024)} %param.23) | copy-start | bytes 49156
  443.7 189.9 %copy-start.43 = (f32[512]{0:T(512)S(1)}, f32[512]{0:T(512)}, u32[]{:S(2)}) copy-start(f32[512]{0:T(512)} %param.33) | copy-start | bytes 6148
  443.7 189.9 %copy-start.44 = (f32[512]{0:T(512)S(1)}, f32[512]{0:T(512)}, u32[]{:S(2)}) copy-start(f32[512]{0:T(512)} %param.32) | copy-start | bytes 6148
  489.3 219.1 %copy-start.4 = (f32[256,512]{1,0:T(8,128)S(1)}, f32[256,512]{1,0:T(8,128)}, u32[]{:S(2)}) copy-start(f32[256,512]{1,0:T(8,128)} %get-tuple-element.145) | copy-start | bytes 1572868
  489.3 219.1 %copy-start.7 = (f32[512]{0:T(512)S(1)}, f32[512]{0:T(512)}, u32[]{:S(2)}) copy-start(f32[512]{0:T(512)} %param.37) | copy-start | bytes 6148
  489.4 219.1 %copy-start.8 = (f32[512]{0:T(512)S(1)}, f32[512]{0:T(512)}, u32[]{:S(2)}) copy-start(f32[512]{0:T(512)} %param.36) | copy-start | bytes 6148
  (27 other events, 106.0 us)
Sparse Core Ops, SparseCore 0:
  8.9 25.2 all-gather.13
  36.3 72.7 all-gather.17
  111.3 71.3 all-gather.19
  184.7 71.3 all-gather.21
  258.0 71.3 all-gather.25
  331.3 71.3 all-gather.27
  404.8 38.8 all-gather.33
  445.8 38.9 all-gather.31
  487.0 71.4 all-gather.15
  560.4 73.1 all-gather.23
  635.6 72.8 all-gather.29
  714.8 29.3 reduce-scatter.1
where the time goes:
time: 751 us
  waiting for transfers between devices  663 us (88%)
  matrix products  41.3 us (5%)
  other arithmetic  16.6 us (2%)
  between operations  14.5 us (2%)
    all_gather x1, waiting for transfers between devices, shards(): lax.all_gather(retention_out_weight, 'sp', axis=1, tiled=True)  75.1 us
    all_gather x1, waiting for transfers between devices, shards(): lax.all_gather(query_weight, 'sp', axis=0, tiled=True)  72.8 us
    all_gather x1, waiting for transfers between devices, shards(): lax.all_gather(key_weight, 'sp', axis=0, tiled=True)  69.2 us
    all_gather x1, waiting for transfers between devices, shards(): lax.all_gather(output_gate_weight, 'sp', axis=0, tiled=True)  69.1 us
    all_gather x1, waiting for transfers between devices, shards(): lax.all_gather(unit_gate_weight, 'sp', axis=0, tiled=True)  68.4 us
    all_gather x1, waiting for transfers between devices, shards(): lax.all_gather(value_weight, 'sp', axis=0, tiled=True)  68 us
    all_gather x1, waiting for transfers between devices, shards(): lax.all_gather(convolution_out_weight, 'sp', axis=1, tiled=True)  66.9 us
    all_gather x1, waiting for transfers between devices, shards(): lax.all_gather(unit_input_weight, 'sp', axis=0, tiled=True)  61 us
  transfers between devices with their start and end apart: 14, of which 13 were waited for; matrix products, arithmetic and copies ran while one was open for 7% of the time, Pallas kernels for 0%

commit v1 on v0

--- a/solution.py
+++ b/solution.py
@@ -238,9 +238,14 @@
         None, :
     ] + channel_bias[None, :]
     convolution_rows = jax.nn.silu(leveled).astype(jnp.bfloat16)
+
+    def switch_rows(body, axis_key, axis_no):
+        now = jax.lax.all_gather(body, axis_key)
+        return jnp.concatenate(now, axis_no)
+
     retention_full, convolution_full = (
         lax.all_gather(retention_out_weight, "sp", axis=1, tiled=True),
-        lax.all_gather(convolution_out_weight, "sp", axis=1, tiled=True),
+        switch_rows(convolution_out_weight, "sp", 1),
     )
     return lax.psum_scatter(
         (

time: 751 us -> 759 us (1.011)
  transfers between devices with their start and end apart: 14 -> 14, of which waited for: 13 -> 12; matrix products, arithmetic and copies ran while one was open for 7% -> 7% of each run, Pallas kernels for 0% -> 0%
where the time goes in v1:
time: 759 us; the launch traced here: 758 us
  waiting for transfers between devices  667 us (88%)
  matrix products  42.2 us (6%)
  between operations  14.3 us (2%)
  other arithmetic  13.5 us (2%)
  local copies, waits for them, and re-layouts  10.7 us (1%)
    all_gather x1, waiting for transfers between devices, shards(): lax.all_gather(retention_out_weight, 'sp', axis=1, tiled=True)  75.3 us
    all_gather x1, waiting for transfers between devices, shards(): lax.all_gather(query_weight, 'sp', axis=0, tiled=True)  72.8 us
    all_gather x1, waiting for transfers between devices, shards(): lax.all_gather(output_gate_weight, 'sp', axis=0, tiled=True)  69.9 us
    all_gather x1, waiting for transfers between devices, shards(): lax.all_gather(key_weight, 'sp', axis=0, tiled=True)  69.2 us
    all_gather x1, waiting for transfers between devices, shards(): lax.all_gather(unit_gate_weight, 'sp', axis=0, tiled=True)  68.4 us
    all_gather x1, waiting for transfers between devices, shards(): lax.all_gather(value_weight, 'sp', axis=0, tiled=True)  67.7 us
    all_gather x1, waiting for transfers between devices, shards(): lax.all_gather(unit_input_weight, 'sp', axis=0, tiled=True)  62.2 us
    all_gather x1, waiting for transfers between devices, switch_rows(): now = jax.lax.all_gather(body, axis_key)  60.9 us
  transfers between devices with their start and end apart: 14, of which 12 were waited for; matrix products, arithmetic and copies ran while one was open for 7% of the time, Pallas kernels for 0%

profile of v1, /device:TPU:0, one launch (start us, length us, event | category | flops | bytes accessed | tf_op | source)
XLA Modules:
  0.0 758.4 jit_solution(10775580775504107831)
XLA Ops:
  13.3 21.0 %all-gather.15.cloned.1.call-done = bf16[256,4096]{1,0:T(8,128)(2,1)} async-done(((bf16[256,1024]{1,0:T(8,128)(2,1)}), bf16[256,4096]{1,0:T(8,128)(2,1)}) %all-gather.15.cloned.1.call-update) | async-done | bytes 2097168 | tf_op jit(solution)/shard_map/all_gather | solution.py:132
  34.2 2.1 fusion.1
  36.3 72.8 %all-gather.19.cloned.1.call-done = bf16[4096,512]{1,0:T(8,128)(2,1)} async-done(((bf16[512,512]{1,0:T(8,128)(2,1)}), bf16[4096,512]{1,0:T(8,128)(2,1)}) %all-gather.19.cloned.1.call-update) | async-done | bytes 4194320 | tf_op jit(solution)/shard_map/all_gather | solution.py:140
  109.2 4.1 fusion.15
  113.5 69.2 %all-gather.21.cloned.1.call-done = bf16[4096,512]{1,0:T(8,128)(2,1)} async-done(((bf16[512,512]{1,0:T(8,128)(2,1)}), bf16[4096,512]{1,0:T(8,128)(2,1)}) %all-gather.21.cloned.1.call-update) | async-done | bytes 4194320 | tf_op jit(solution)/shard_map/all_gather | solution.py:141
  182.7 4.1 fusion.14
  188.4 67.7 %all-gather.23.cloned.1.call-done = bf16[4096,512]{1,0:T(8,128)(2,1)} async-done(((bf16[512,512]{1,0:T(8,128)(2,1)}), bf16[4096,512]{1,0:T(8,128)(2,1)}) %all-gather.23.cloned.1.call-update) | async-done | bytes 4194320 | tf_op jit(solution)/shard_map/all_gather | solution.py:142
  256.0 4.1 convolution_convert_fusion.2
  262.2 0.8 convolution_bitcast_fusion.1
  267.2 62.2 %all-gather.27.cloned.1.call-done = bf16[4096,512]{1,0:T(8,128)(2,1)} async-done(((bf16[512,512]{1,0:T(8,128)(2,1)}), bf16[4096,512]{1,0:T(8,128)(2,1)}) %all-gather.27.cloned.1.call-update) | async-done | bytes 4194320 | tf_op jit(solution)/shard_map/all_gather | solution.py:144
  329.4 4.9 fusion.13
  334.3 68.4 %all-gather.29.cloned.1.call-done = bf16[4096,512]{1,0:T(8,128)(2,1)} async-done(((bf16[512,512]{1,0:T(8,128)(2,1)}), bf16[4096,512]{1,0:T(8,128)(2,1)}) %all-gather.29.cloned.1.call-update) | async-done | bytes 4194320 | tf_op jit(solution)/shard_map/all_gather | solution.py:145
  402.7 4.3 fusion.12
  407.1 2.6 collective-permute-start
  409.7 1.5 collective-permute-start.1
  413.4 0.8 convolution_add_fusion.2
  414.4 0.7 rev.15
  415.3 60.9 %all-gather.35.cloned.1.call-done = bf16[4096,512]{1,0:T(8,128)(2,1)} async-done(((bf16[512,512]{1,0:T(8,128)(2,1)}), bf16[4096,512]{1,0:T(8,128)(2,1)}) %all-gather.35.cloned.1.call-update) | async-done | bytes 4194320 | tf_op jit(solution)/shard_map/all_gather | solution.py:243
  476.4 6.5 copy.84
  483.0 3.2 fusion.96
  486.2 5.9 all-reduce
  492.1 25.1 %all-gather.33.cloned.1.call-done = bf16[32,128,128]{2,1,0:T(8,128)(2,1)} async-done(((bf16[4,128,128]{2,1,0:T(8,128)(2,1)}), bf16[32,128,128]{2,1,0:T(8,128)(2,1)}) %all-gather.33.cloned.1.call-update) | async-done | bytes 1048592 | tf_op jit(solution)/shard_map/all_gather | solution.py:173
  517.2 1.6 multiply_reduce_fusion
  518.8 39.6 %all-gather.31.cloned.1.call-done = bf16[32,128,128]{2,1,0:T(8,128)(2,1)} async-done(((bf16[4,128,128]{2,1,0:T(8,128)(2,1)}), bf16[32,128,128]{2,1,0:T(8,128)(2,1)}) %all-gather.31.cloned.1.call-update) | async-done | bytes 1048592 | tf_op jit(solution)/shard_map/all_gather | solution.py:170
  558.3 1.6 multiply_reduce_fusion.1
  559.9 0.8 fusion.17
  560.7 0.8 fusion.104
  561.9 69.9 %all-gather.17.cloned.1.call-done = bf16[4096,512]{1,0:T(8,128)(2,1)} async-done(((bf16[512,512]{1,0:T(8,128)(2,1)}), bf16[4096,512]{1,0:T(8,128)(2,1)}) %all-gather.17.cloned.1.call-update) | async-done | bytes 4194320 | tf_op jit(solution)/shard_map/all_gather | solution.py:143
  631.9 75.3 %all-gather.25.cloned.1.call-done = bf16[512,4096]{1,0:T(8,128)(2,1)} async-done(((bf16[512,512]{1,0:T(8,128)(2,1)}), bf16[512,4096]{1,0:T(8,128)(2,1)}) %all-gather.25.cloned.1.call-update) | async-done | bytes 4194320 | tf_op jit(solution)/shard_map/all_gather | solution.py:247
  707.1 8.7 %fusion.28 = f32[256,4096]{1,0:T(8,128)} fusion(bf16[512,4096]{1,0:T(8,128)(2,1)} %all-gather.25.cloned.1.call-done, f32[256,512]{1,0:T(8,128)S(1)} %copy.105, bf16[4096,512]{1,0:T(8,128)(2,1)} %all-gather.17.cloned.1.call-done, f32[512]{0:T(512)S(1)} %copy-done.29, f32[512]{0:T(512)S(1)} %copy-done.30, ...), kind=kOutput, calls=%fused_computation.89 | convolution fusion | flops 2152988672 | bytes 15225856 | tf_op jit(solution)/shard_map/dot_general | solution.py:252
  715.8 6.2 fusion
  722.0 29.5 %reduce-scatter.2.cloned.1.call-done = bf16[64,4096]{1,0:T(8,128)(2,1)} async-done(((bf16[256,4096]{1,0:T(8,128)(2,1)}), bf16[64,4096]{1,0:T(8,128)(2,1)}) %reduce-scatter.2.cloned.1.call-update) | async-done | bytes 524304 | tf_op jit(solution)/shard_map/reduce_scatter | solution.py:250
  (156 shorter events, 17.8 us)
Async XLA Ops:
  6.5 102.6 %copy-start.27 = (f32[4096]{0:T(1024)S(1)}, f32[4096]{0:T(1024)}, u32[]{:S(2)}) copy-start(f32[4096]{0:T(1024)} %param.23) | copy-start | bytes 49156
  6.5 27.7 %all-gather.15.cloned.1.call-start = ((), (), s32[]{:S(2)}) async-start(), calls=%async_computation.1 | async-start | bytes 2621440 | tf_op jit(solution)/shard_map/all_gather | solution.py:132
  7.3 101.9 %all-gather.19.cloned.1.call-start = ((), (), s32[]{:S(2)}) async-start(), calls=%async_computation.3 | async-start | bytes 4718592 | tf_op jit(solution)/shard_map/all_gather | solution.py:140
  8.0 174.7 %all-gather.21.cloned.1.call-start = ((), (), s32[]{:S(2)}) async-start(), calls=%async_computation.4 | async-start | bytes 4718592 | tf_op jit(solution)/shard_map/all_gather | solution.py:141
  8.7 247.3 %all-gather.23.cloned.1.call-start = ((), (), s32[]{:S(2)}) async-start(), calls=%async_computation.5 | async-start | bytes 4718592 | tf_op jit(solution)/shard_map/all_gather | solution.py:142
  9.3 320.1 %all-gather.27.cloned.1.call-start = ((), (), s32[]{:S(2)}) async-start(), calls=%async_computation.7 | async-start | bytes 4718592 | tf_op jit(solution)/shard_map/all_gather | solution.py:144
  9.9 392.8 %all-gather.29.cloned.1.call-start = ((), (), s32[]{:S(2)}) async-start(), calls=%async_computation.8 | async-start | bytes 4718592 | tf_op jit(solution)/shard_map/all_gather | solution.py:145
  10.5 465.7 %all-gather.35.cloned.1.call-start = ((), (), s32[]{:S(2)}) async-start(), calls=%async_computation.12 | async-start | bytes 4718592 | tf_op jit(solution)/shard_map/all_gather | solution.py:243
  11.2 506.0 %all-gather.33.cloned.1.call-start = ((), (), s32[]{:S(2)}) async-start(), calls=%async_computation.11 | async-start | bytes 1179648 | tf_op jit(solution)/shard_map/all_gather | solution.py:173
  36.3 366.4 %copy-start.25 = (f32[256]{0:T(256)}, f32[256]{0:T(256)S(1)}, u32[]{:S(2)}) copy-start(f32[256]{0:T(256)S(1)} %add_rsqrt_fusion.2) | copy-start | bytes 3076
  262.0 296.3 %all-gather.31.cloned.1.call-start = ((), (), s32[]{:S(2)}) async-start(), calls=%async_computation.10 | async-start | bytes 1179648 | tf_op jit(solution)/shard_map/all_gather | solution.py:170
  264.0 367.8 %all-gather.17.cloned.1.call-start = ((), (), s32[]{:S(2)}) async-start(), calls=%async_computation.2 | async-start | bytes 4718592 | tf_op jit(solution)/shard_map/all_gather | solution.py:143
  264.6 442.5 %all-gather.25.cloned.1.call-start = ((), (), s32[]{:S(2)}) async-start(), calls=%async_computation.6 | async-start | bytes 4718592 | tf_op jit(solution)/shard_map/all_gather | solution.py:247
  265.4 486.2 %reduce-scatter.2.cloned.1.call-start = ((), (), s32[]{:S(2)}) async-start(), calls=%async_computation.9 | async-start | bytes 2621440 | tf_op jit(solution)/shard_map/reduce_scatter | solution.py:250
  407.0 7.1 copy-start.2
  407.1 75.8 %collective-permute-start = (bf16[15,512]{1,0:T(8,128)(2,1)S(1)}, bf16[15,512]{1,0:T(8,128)(2,1)S(1)}, u32[]{:S(2)}, u32[]{:S(2)}) collective-permute-start(bf16[15,512]{1,0:T(8,128)(2,1)S(1)} %get-tuple-element.178), channel_id=1, source_target_pairs={{0,4},{4,8},{8,12},{12,16},{16,20},{20,24},{24,28},{1,5},{5,9},{9,... | collective-permute-start | bytes 46088 | tf_op jit(solution)/shard_map/ppermute | solution.py:22
  409.7 73.2 %collective-permute-start.1 = (bf16[15,512]{1,0:T(8,128)(2,1)S(1)}, bf16[15,512]{1,0:T(8,128)(2,1)S(1)}, u32[]{:S(2)}, u32[]{:S(2)}) collective-permute-start(bf16[15,512]{1,0:T(8,128)(2,1)S(1)} %get-tuple-element.179), channel_id=1, source_target_pairs={{4,0},{8,4},{12,8},{16,12},{20,16},{24,20},{28,24},{5,1},{9,5},{13... | collective-permute-start | bytes 46088 | tf_op jit(solution)/shard_map/ppermute | solution.py:24
  476.2 6.7 copy-start.9
  476.3 6.7 copy-start.10
  476.3 6.7 copy-start.11
  476.3 6.7 copy-start.12
  476.3 6.7 copy-start.13
  476.3 6.7 copy-start.14
  476.3 6.7 copy-start.15
  476.3 6.7 copy-start.16
  476.3 6.7 copy-start.17
  517.2 189.9 %copy-start.26 = (f32[256]{0:T(256)S(1)}, f32[256]{0:T(256)}, u32[]{:S(2)}) copy-start(f32[256]{0:T(256)} %copy-done.25) | copy-start | bytes 3076
  517.2 189.9 %copy-start.28 = (f32[4096]{0:T(1024)S(1)}, f32[4096]{0:T(1024)}, u32[]{:S(2)}) copy-start(f32[4096]{0:T(1024)} %param.23) | copy-start | bytes 49156
  517.2 189.9 %copy-start.29 = (f32[512]{0:T(512)S(1)}, f32[512]{0:T(512)}, u32[]{:S(2)}) copy-start(f32[512]{0:T(512)} %param.33) | copy-start | bytes 6148
  517.2 189.9 %copy-start.30 = (f32[512]{0:T(512)S(1)}, f32[512]{0:T(512)}, u32[]{:S(2)}) copy-start(f32[512]{0:T(512)} %param.32) | copy-start | bytes 6148
  561.9 153.9 %copy-start.23 = (f32[512]{0:T(512)S(1)}, f32[512]{0:T(512)}, u32[]{:S(2)}) copy-start(f32[512]{0:T(512)} %param.37) | copy-start | bytes 6148
  561.9 153.9 %copy-start.24 = (f32[512]{0:T(512)S(1)}, f32[512]{0:T(512)}, u32[]{:S(2)}) copy-start(f32[512]{0:T(512)} %param.36) | copy-start | bytes 6148
  (13 other events, 74.7 us)
Sparse Core Ops, SparseCore 0:
  8.9 25.2 all-gather.14
  36.3 72.7 all-gather.18
  111.3 71.3 all-gather.20
  184.7 71.3 all-gather.22
  258.0 71.3 all-gather.26
  331.4 71.3 all-gather.28
  404.9 71.3 all-gather.34
  478.4 38.7 all-gather.32
  519.3 38.9 all-gather.30
  560.3 71.4 all-gather.16
  633.9 73.1 all-gather.24
  722.2 29.3 reduce-scatter.1
